TPU v7x, 128 devices: a whole 4x4x4 slice. The times are simulated.
128 devices in a mesh: fs: 16 (over z, x), tp: 8 (over y, core).
Axes of the slice: x: 4, y: 4, z: 4, core: 2. Of those that a mesh axis runs over, the one named last changes fastest.
Arguments:
- tokens: bfloat16 [32, 384, 2048], P('fs', None, 'tp'), may hold values from -20 to 20
- first_gain: float32 [2048], replicated, may hold values from 0.1 to 1.9
- first_gate: bfloat16 [2048, 5120], P('fs', 'tp'), may hold values from -0.125 to 0.125
- first_up: bfloat16 [2048, 5120], P('fs', 'tp'), may hold values from -0.125 to 0.125
- first_down: bfloat16 [5120, 2048], P('tp', 'fs'), may hold values from -0.078125 to 0.078125
- mixer_gain: float32 [2048], replicated, may hold values from 0.1 to 1.9
- conv_input: bfloat16 [2048, 1024], P('fs', 'tp'), may hold values from -0.125 to 0.125
- outer_gate: bfloat16 [2048, 1024], P('fs', 'tp'), may hold values from -0.125 to 0.125
- inner_gate: bfloat16 [2048, 1024], P('fs', 'tp'), may hold values from -0.125 to 0.125
- conv_taps: float32 [3, 1024], P(None, 'tp'), may hold values from -3.5 to 3.5
- mixer_out: bfloat16 [1024, 2048], P('tp', 'fs'), may hold values from -0.1875 to 0.1875
- second_gain: float32 [2048], replicated, may hold values from 0.1 to 1.9
- second_gate: bfloat16 [2048, 5120], P('fs', 'tp'), may hold values from -0.125 to 0.125
- second_up: bfloat16 [2048, 5120], P('fs', 'tp'), may hold values from -0.125 to 0.125
- second_down: bfloat16 [5120, 2048], P('tp', 'fs'), may hold values from -0.078125 to 0.078125
Outputs:
- layer_out: bfloat16 [32, 384, 2048], P('fs', None, 'tp')
All inputs are finite; a program needn't handle non-finite values.
Results may differ from a plain program's by a relative error of at most 0.015.
Values may be sent and summed in bfloat16 or wider, within the bound.
A program may use at most 64 MiB of HBM per device.

v0:
```python
import jax
import jax.numpy as jnp
from jax import lax
from jax.sharding import PartitionSpec as P

epsilon = 1e-05


def sent_together(arrays, axis, dim, along):
    ends, at = ([], 0)
    for a in arrays[:-1]:
        at += a.shape[along]
        ends.append(at)
    both = jnp.concatenate(arrays, axis=along)
    return tuple(jnp.split(lax.all_gather(both, axis, axis=dim, tiled=True), ends, axis=along))


def copy_for_each(value, axis):
    copies = jnp.broadcast_to(value, (lax.axis_size(axis), *value.shape))
    return lax.all_to_all(copies, axis, split_axis=0, concat_axis=0, tiled=True)


def joined_along(pieces, dim):
    shape = list(pieces.shape[1:])
    shape[dim] *= pieces.shape[0]
    return jnp.moveaxis(pieces, 0, dim).reshape(shape)


def gathered_copies(value, axis, dim):
    pieces = copy_for_each(value, axis)
    return joined_along(pieces, dim)


def norm_rows(stream, gain):
    whole = lax.all_gather(stream, "tp", axis=1, tiled=True)
    values = whole.astype(jnp.float32)
    scale = lax.rsqrt(jnp.mean(values * values, axis=1, keepdims=True) + epsilon)
    return (values * scale * gain).astype(jnp.bfloat16)


def add_rows(gathered, piece):
    return jnp.dot(gathered, piece, preferred_element_type=jnp.float32)


def ffn_inputs(gathered, gate_weight, up_weight):
    pieces = sent_together((gate_weight, up_weight), "fs", 0, 1)
    gate = add_rows(gathered, pieces[0])
    upward = add_rows(gathered, pieces[1])
    return (gate, upward)


def mixer_inputs(gathered, conv_input, outer_gate, inner_gate):
    pieces = sent_together((conv_input, outer_gate, inner_gate), "fs", 0, 1)
    conv_values = add_rows(gathered, pieces[0])
    outer = add_rows(gathered, pieces[1])
    inner = add_rows(gathered, pieces[2])
    return (conv_values, outer, inner)


def project_down(hidden, weight):
    partial_sum = jnp.dot(
        hidden, gathered_copies(weight, "fs", 1), preferred_element_type=jnp.float32
    )
    result = lax.psum_scatter(
        partial_sum.astype(jnp.bfloat16), "tp", scatter_dimension=1, tiled=True
    ).astype(jnp.float32)
    return result


def half_ffn(stream, gain, gate_weight, up_weight, down_weight):
    gathered = norm_rows(stream, gain)
    gate, upward = ffn_inputs(gathered, gate_weight, up_weight)
    hidden = (jax.nn.silu(gate) * upward).astype(jnp.bfloat16)
    branch = project_down(hidden, down_weight)
    return (stream.astype(jnp.float32) + 0.5 * branch).astype(jnp.bfloat16)


def conv_mixer(stream, seqs, gain, conv_input, outer_gate, inner_gate, conv_taps, mixer_out):
    gathered = norm_rows(stream, gain)
    conv_values, outer, inner = mixer_inputs(gathered, conv_input, outer_gate, inner_gate)
    gated_input = (inner * conv_values).reshape(seqs, -1, conv_values.shape[1])
    one_back = jnp.pad(gated_input, ((0, 0), (1, 0), (0, 0)))[:, :-1]
    two_back = jnp.pad(gated_input, ((0, 0), (2, 0), (0, 0)))[:, :-2]
    convolved = conv_taps[0] * two_back + conv_taps[1] * one_back + conv_taps[2] * gated_input
    mixed = (outer * convolved.reshape(conv_values.shape)).astype(jnp.bfloat16)
    branch = project_down(mixed, mixer_out)
    return (stream.astype(jnp.float32) + branch).astype(jnp.bfloat16)


def on_device(
    tokens,
    first_gain,
    first_gate,
    first_up,
    first_down,
    mixer_gain,
    conv_input,
    outer_gate,
    inner_gate,
    conv_taps,
    mixer_out,
    second_gain,
    second_gate,
    second_up,
    second_down,
):
    seqs, length, width = tokens.shape
    stream = tokens.reshape(seqs * length, width)
    stream = half_ffn(stream, first_gain, first_gate, first_up, first_down)
    stream = conv_mixer(
        stream, seqs, mixer_gain, conv_input, outer_gate, inner_gate, conv_taps, mixer_out
    )
    stream = half_ffn(stream, second_gain, second_gate, second_up, second_down)
    return stream.reshape(seqs, length, width)


def solution(mesh):
    in_specs = (
        P("fs", None, "tp"),
        P(),
        P("fs", "tp"),
        P("fs", "tp"),
        P("tp", "fs"),
        P(),
        P("fs", "tp"),
        P("fs", "tp"),
        P("fs", "tp"),
        P(None, "tp"),
        P("tp", "fs"),
        P(),
        P("fs", "tp"),
        P("fs", "tp"),
        P("tp", "fs"),
    )
    out_specs = P("fs", None, "tp")
    return jax.shard_map(
        on_device, mesh=mesh, in_specs=in_specs, out_specs=out_specs, check_vma=False
    )
```

profile of v0, /device:TPU:0, one launch (start us, length us, event | category | flops | bytes accessed | tf_op | source)
XLA Modules:
  0.0 431.1 jit_solution(13457404551450091952)
XLA Ops:
  10.1 1.9 broadcast_in_dim.6
  12.0 8.2 %all-to-all-start = ((bf16[16,640,128]{1,2,0:T(8,128)(2,1)}), bf16[16,640,128]{1,2,0:T(8,128)(2,1)}, u32[]{:S(2)}, u32[]{:S(2)}) async-start(bf16[16,640,128]{1,2,0:T(8,128)(2,1)} %broadcast_in_dim.6), calls=%async_computation | async-start | bytes 5242880 | tf_op jit(solution)/shard_map/all_to_all | solution.py:20
  20.3 22.4 %all-gather.7.cloned.1.call-done = bf16[768,2048]{1,0:T(8,128)(2,1)} async-done(((bf16[768,256]{1,0:T(8,128)(2,1)}), bf16[768,2048]{1,0:T(8,128)(2,1)}) %all-gather.7.cloned.1.call-update) | async-done | bytes 3145744 | tf_op jit(solution)/shard_map/all_gather | solution.py:35
  42.7 2.7 fusion
  45.4 56.7 %all-gather.9.cloned.1.call-done = bf16[2048,1280]{1,0:T(8,128)(2,1)} async-done(((bf16[128,1280]{1,0:T(8,128)(2,1)}), bf16[2048,1280]{1,0:T(8,128)(2,1)}) %all-gather.9.cloned.1.call-update) | async-done | bytes 5242896 | tf_op jit(solution)/shard_map/all_gather | solution.py:15
  102.1 5.7 %fusion.15 = f32[768,640]{1,0:T(8,128)} fusion(bf16[2048,1280]{1,0:T(8,128)(2,1)} %all-gather.9.cloned.1.call-done, bf16[768,2048]{1,0:T(8,128)(2,1)S(1)} %copy-done.3, f32[2048]{0:T(1024)S(1)} %copy-done.15, f32[768]{0:T(1024)S(1)} %add_rsqrt_fusion.2), kind=kOutput, calls=%fused_computation.24 | convolution fusion | flops 2019557376 | bytes 7744512 | tf_op jit(solution)/shard_map/dot_general | solution.py:42
  107.8 10.7 %convolution_convert_fusion.1 = bf16[768,2048]{1,0:T(8,128)(2,1)} fusion(bf16[640,2048]{0,1:T(8,128)(2,1)} %bitcast.2, f32[768,640]{1,0:T(8,128)} %fusion.15, bf16[2048,1280]{1,0:T(8,128)(2,1)} %all-gather.9.cloned.1.call-done, bf16[768,2048]{1,0:T(8,128)(2,1)S(1)} %copy-done.3, f32[2048]{0:T(1024)S(1)} %copy-done.15, f32[768]{0:T(1024)S(1)} %add_rsqrt_fusion.2), kind=kOutput, calls=%fused_computation.16 | convolution fusion | flops 4037345280 | bytes 13511680 | tf_op jit(solution)/shard_map/dot_general | solution.py:61
  118.6 35.6 %reduce-scatter.4.cloned.1.call-done = bf16[768,256]{1,0:T(8,128)(2,1)} async-done(((bf16[768,2048]{1,0:T(8,128)(2,1)}), bf16[768,256]{1,0:T(8,128)(2,1)}) %reduce-scatter.4.cloned.1.call-update) | async-done | bytes 393232 | tf_op jit(solution)/shard_map/reduce_scatter | solution.py:64
  157.9 7.0 %all-to-all-start.1 = ((bf16[16,128,128]{1,2,0:T(8,128)(2,1)}), bf16[16,128,128]{1,2,0:T(8,128)(2,1)}, u32[]{:S(2)}, u32[]{:S(2)}) async-start(bf16[16,128,128]{1,2,0:T(8,128)(2,1)} %broadcast_in_dim.7), calls=%async_computation.2 | async-start | bytes 1048576 | tf_op jit(solution)/shard_map/all_to_all | solution.py:20
  165.2 21.0 %all-gather.11.cloned.1.call-done = bf16[768,2048]{1,0:T(8,128)(2,1)} async-done(((bf16[768,256]{1,0:T(8,128)(2,1)}), bf16[768,2048]{1,0:T(8,128)(2,1)}) %all-gather.11.cloned.1.call-update) | async-done | bytes 3145744 | tf_op jit(solution)/shard_map/all_gather | solution.py:35
  186.2 2.7 fusion.3
  189.8 43.1 %all-gather.13.cloned.1.call-done = bf16[2048,384]{1,0:T(8,128)(2,1)} async-done(((bf16[128,384]{1,0:T(8,128)(2,1)}), bf16[2048,384]{1,0:T(8,128)(2,1)}) %all-gather.13.cloned.1.call-update) | async-done | bytes 1572880 | tf_op jit(solution)/shard_map/all_gather | solution.py:15
  233.0 2.0 fusion.35
  235.0 2.0 convolution_multiply_fusion
  237.1 6.2 %convolution_convert_fusion.2 = bf16[768,2048]{1,0:T(8,128)(2,1)} fusion(bf16[128,2048]{0,1:T(8,128)(2,1)} %bitcast.9, f32[768,128]{1,0:T(8,128)S(1)} %bitcast.28, bf16[768,2048]{1,0:T(8,128)(2,1)S(1)} %fusion.5, bf16[2048,384]{1,0:T(8,128)(2,1)} %all-gather.13.cloned.1.call-done), kind=kOutput, calls=%fused_computation.17 | convolution fusion | flops 807075840 | bytes 7733248 | tf_op jit(solution)/shard_map/dot_general | solution.py:61
  243.4 35.3 %reduce-scatter.6.cloned.1.call-done = bf16[768,256]{1,0:T(8,128)(2,1)} async-done(((bf16[768,2048]{1,0:T(8,128)(2,1)}), bf16[768,256]{1,0:T(8,128)(2,1)}) %reduce-scatter.6.cloned.1.call-update) | async-done | bytes 393232 | tf_op jit(solution)/shard_map/reduce_scatter | solution.py:64
  281.6 1.9 broadcast_in_dim.8
  283.5 7.1 %all-to-all-start.2 = ((bf16[16,640,128]{1,2,0:T(8,128)(2,1)}), bf16[16,640,128]{1,2,0:T(8,128)(2,1)}, u32[]{:S(2)}, u32[]{:S(2)}) async-start(bf16[16,640,128]{1,2,0:T(8,128)(2,1)} %broadcast_in_dim.8), calls=%async_computation.4 | async-start | bytes 5242880 | tf_op jit(solution)/shard_map/all_to_all | solution.py:20
  290.9 19.8 %all-gather.15.cloned.1.call-done = bf16[768,2048]{1,0:T(8,128)(2,1)} async-done(((bf16[768,256]{1,0:T(8,128)(2,1)}), bf16[768,2048]{1,0:T(8,128)(2,1)}) %all-gather.15.cloned.1.call-update) | async-done | bytes 3145744 | tf_op jit(solution)/shard_map/all_gather | solution.py:35
  310.7 2.7 fusion.6
  313.4 57.2 %all-gather.17.cloned.1.call-done = bf16[2048,1280]{1,0:T(8,128)(2,1)} async-done(((bf16[128,1280]{1,0:T(8,128)(2,1)}), bf16[2048,1280]{1,0:T(8,128)(2,1)}) %all-gather.17.cloned.1.call-update) | async-done | bytes 5242896 | tf_op jit(solution)/shard_map/all_gather | solution.py:15
  370.6 5.7 %fusion.11 = f32[768,640]{1,0:T(8,128)} fusion(bf16[2048,1280]{1,0:T(8,128)(2,1)} %all-gather.17.cloned.1.call-done, bf16[768,2048]{1,0:T(8,128)(2,1)S(1)} %copy-done.4, f32[2048]{0:T(1024)S(1)} %copy-done.16, f32[768]{0:T(1024)S(1)} %add_rsqrt_fusion), kind=kOutput, calls=%fused_computation.20 | convolution fusion | flops 2019557376 | bytes 7744512 | tf_op jit(solution)/shard_map/dot_general | solution.py:42
  376.3 10.7 %convolution_convert_fusion = bf16[768,2048]{1,0:T(8,128)(2,1)} fusion(bf16[640,2048]{0,1:T(8,128)(2,1)} %bitcast.11, f32[768,640]{1,0:T(8,128)} %fusion.11, bf16[2048,1280]{1,0:T(8,128)(2,1)} %all-gather.17.cloned.1.call-done, bf16[768,2048]{1,0:T(8,128)(2,1)S(1)} %copy-done.4, f32[2048]{0:T(1024)S(1)} %copy-done.16, f32[768]{0:T(1024)S(1)} %add_rsqrt_fusion), kind=kOutput, calls=%fused_computation.15 | convolution fusion | flops 4037345280 | bytes 13511680 | tf_op jit(solution)/shard_map/dot_general | solution.py:61
  387.0 35.7 %reduce-scatter.8.cloned.1.call-done = bf16[768,256]{1,0:T(8,128)(2,1)} async-done(((bf16[768,2048]{1,0:T(8,128)(2,1)}), bf16[768,256]{1,0:T(8,128)(2,1)}) %reduce-scatter.8.cloned.1.call-update) | async-done | bytes 393232 | tf_op jit(solution)/shard_map/reduce_scatter | solution.py:64
  (71 shorter events, 13.6 us)
Async XLA Ops:
  6.5 36.1 %all-gather.7.cloned.1.call-start = ((), (), s32[]{:S(2)}) async-start(), calls=%async_computation.6 | async-start | bytes 3538944 | tf_op jit(solution)/shard_map/all_gather | solution.py:35
  7.3 94.8 %all-gather.9.cloned.1.call-start = ((), (), s32[]{:S(2)}) async-start(), calls=%async_computation.7 | async-start | bytes 5570560 | tf_op jit(solution)/shard_map/all_gather | solution.py:15
  12.0 90.1 %copy-start.15 = (f32[2048]{0:T(1024)S(1)}, f32[2048]{0:T(1024)}, u32[]{:S(2)}) copy-start(f32[2048]{0:T(1024)} %param.16) | copy-start | bytes 24580
  12.0 95.8 %all-to-all-start = ((bf16[16,640,128]{1,2,0:T(8,128)(2,1)}), bf16[16,640,128]{1,2,0:T(8,128)(2,1)}, u32[]{:S(2)}, u32[]{:S(2)}) async-start(bf16[16,640,128]{1,2,0:T(8,128)(2,1)} %broadcast_in_dim.6), calls=%async_computation | async-start | bytes 5242880 | tf_op jit(solution)/shard_map/all_to_all | solution.py:20
  20.2 134.0 %reduce-scatter.4.cloned.1.call-start = ((), (), s32[]{:S(2)}) async-start(), calls=%async_computation.8 | async-start | bytes 3538944 | tf_op jit(solution)/shard_map/reduce_scatter | solution.py:64
  42.7 59.5 %copy-start.3 = (bf16[768,2048]{1,0:T(8,128)(2,1)S(1)}, bf16[768,2048]{1,0:T(8,128)(2,1)}, u32[]{:S(2)}) copy-start(bf16[768,2048]{1,0:T(8,128)(2,1)} %all-gather.7.cloned.1.call-done) | copy-start | bytes 9437188
  118.5 37.7 %copy-start.10 = (bf16[128,128]{1,0:T(8,128)(2,1)S(1)}, bf16[128,128]{1,0:T(8,128)(2,1)}, u32[]{:S(2)}) copy-start(bf16[128,128]{1,0:T(8,128)(2,1)} %param.23) | copy-start | bytes 98308
  118.5 37.7 %copy-start.11 = (bf16[128,128]{1,0:T(8,128)(2,1)S(1)}, bf16[128,128]{1,0:T(8,128)(2,1)}, u32[]{:S(2)}) copy-start(bf16[128,128]{1,0:T(8,128)(2,1)} %param.22) | copy-start | bytes 98308
  118.5 37.7 %copy-start.12 = (bf16[128,128]{1,0:T(8,128)(2,1)S(1)}, bf16[128,128]{1,0:T(8,128)(2,1)}, u32[]{:S(2)}) copy-start(bf16[128,128]{1,0:T(8,128)(2,1)} %param.21) | copy-start | bytes 98308
  118.5 38.3 %copy-start.9 = (bf16[128,128]{1,0:T(8,128)(2,1)S(1)}, bf16[128,128]{1,0:T(8,128)(2,1)}, u32[]{:S(2)}) copy-start(bf16[128,128]{1,0:T(8,128)(2,1)} %param.25) | copy-start | bytes 98308
  118.5 46.6 %copy-start.14 = (f32[3,128]{1,0:T(4,128)S(1)}, f32[3,128]{1,0:T(4,128)}, u32[]{:S(2)}) copy-start(f32[3,128]{1,0:T(4,128)} %param.24) | copy-start | bytes 4612
  118.5 70.4 %copy-start.13 = (f32[2048]{0:T(1024)S(1)}, f32[2048]{0:T(1024)}, u32[]{:S(2)}) copy-start(f32[2048]{0:T(1024)} %param.20) | copy-start | bytes 24580
  118.6 67.6 %all-gather.11.cloned.1.call-start = ((), (), s32[]{:S(2)}) async-start(), calls=%async_computation.9 | async-start | bytes 3538944 | tf_op jit(solution)/shard_map/all_gather | solution.py:35
  156.1 76.9 %all-gather.13.cloned.1.call-start = ((), (), s32[]{:S(2)}) async-start(), calls=%async_computation.10 | async-start | bytes 1671168 | tf_op jit(solution)/shard_map/all_gather | solution.py:15
  157.9 79.2 %all-to-all-start.1 = ((bf16[16,128,128]{1,2,0:T(8,128)(2,1)}), bf16[16,128,128]{1,2,0:T(8,128)(2,1)}, u32[]{:S(2)}, u32[]{:S(2)}) async-start(bf16[16,128,128]{1,2,0:T(8,128)(2,1)} %broadcast_in_dim.7), calls=%async_computation.2 | async-start | bytes 1048576 | tf_op jit(solution)/shard_map/all_to_all | solution.py:20
  164.9 113.8 %reduce-scatter.6.cloned.1.call-start = ((), (), s32[]{:S(2)}) async-start(), calls=%async_computation.11 | async-start | bytes 3538944 | tf_op jit(solution)/shard_map/reduce_scatter | solution.py:64
  243.3 37.3 %copy-start.7 = (bf16[128,640]{1,0:T(8,128)(2,1)S(1)}, bf16[128,640]{1,0:T(8,128)(2,1)}, u32[]{:S(2)}) copy-start(bf16[128,640]{1,0:T(8,128)(2,1)} %param.27) | copy-start | bytes 491524
  243.3 38.1 %copy-start.8 = (bf16[640,128]{1,0:T(8,128)(2,1)S(1)}, bf16[640,128]{1,0:T(8,128)(2,1)}, u32[]{:S(2)}) copy-start(bf16[640,128]{1,0:T(8,128)(2,1)} %param.29) | copy-start | bytes 491524
  243.3 67.3 %all-gather.15.cloned.1.call-start = ((), (), s32[]{:S(2)}) async-start(), calls=%async_computation.12 | async-start | bytes 3538944 | tf_op jit(solution)/shard_map/all_gather | solution.py:35
  280.6 90.0 %all-gather.17.cloned.1.call-start = ((), (), s32[]{:S(2)}) async-start(), calls=%async_computation.13 | async-start | bytes 5570560 | tf_op jit(solution)/shard_map/all_gather | solution.py:15
  283.5 87.1 %copy-start.16 = (f32[2048]{0:T(1024)S(1)}, f32[2048]{0:T(1024)}, u32[]{:S(2)}) copy-start(f32[2048]{0:T(1024)} %param.26) | copy-start | bytes 24580
  283.5 92.8 %all-to-all-start.2 = ((bf16[16,640,128]{1,2,0:T(8,128)(2,1)}), bf16[16,640,128]{1,2,0:T(8,128)(2,1)}, u32[]{:S(2)}, u32[]{:S(2)}) async-start(bf16[16,640,128]{1,2,0:T(8,128)(2,1)} %broadcast_in_dim.8), calls=%async_computation.4 | async-start | bytes 5242880 | tf_op jit(solution)/shard_map/all_to_all | solution.py:20
  290.6 132.1 %reduce-scatter.8.cloned.1.call-start = ((), (), s32[]{:S(2)}) async-start(), calls=%async_computation.14 | async-start | bytes 3538944 | tf_op jit(solution)/shard_map/reduce_scatter | solution.py:64
  310.7 60.0 %copy-start.4 = (bf16[768,2048]{1,0:T(8,128)(2,1)S(1)}, bf16[768,2048]{1,0:T(8,128)(2,1)}, u32[]{:S(2)}) copy-start(bf16[768,2048]{1,0:T(8,128)(2,1)} %all-gather.15.cloned.1.call-done) | copy-start | bytes 9437188
  (5 other events, 147.0 us)
Sparse Core Ops, SparseCore 0:
  9.0 33.5 all-gather.6
  44.8 57.2 all-gather.8
  118.7 35.4 reduce-scatter.3
  156.2 29.9 all-gather.10
  188.2 44.7 all-gather.12
  243.5 35.2 reduce-scatter.5
  280.7 29.9 all-gather.14
  312.8 57.7 all-gather.16
  387.1 35.4 reduce-scatter.7
where the time goes:
time: 432 us; the launch traced here: 431 us
  waiting for transfers between devices  328 us (76%)
  matrix products  42.9 us (10%)
  starting transfers between devices  23 us (5%)
  other arithmetic  17.8 us (4%)
  between operations  13.4 us (3%)
  local copies, waits for them, and re-layouts  6.23 us (1%)
    all_gather x3, waiting for transfers between devices, sent_together(): lax.all_gather(both, axis, axis=dim, tiled=True)  157 us
    reduce_scatter x3, waiting for transfers between devices, project_down(): lax.psum_scatter(partial_sum.astype(jnp.bfloat16), 'tp', scatter_dimensio...  107 us
    all_gather x3, waiting for transfers between devices, norm_rows(): whole = lax.all_gather(stream, 'tp', axis=1, tiled=True)  63.2 us
    dot_general x3, matrix products, project_down(): jnp.dot(hidden, gathered_copies(weight, 'fs', 1), preferred_element_type=...  27.5 us
    all_to_all x3, starting transfers between devices, copy_for_each(): return lax.all_to_all(copies, axis, split_axis=0, concat_axis=0, tiled=True)  22.3 us
    dot_general x4, matrix products, add_rows(): return jnp.dot(gathered, piece, preferred_element_type=jnp.float32)  15.4 us
  transfers between devices with their start and end apart: 12, of which 9 were waited for; matrix products, arithmetic and copies ran while one was open for 8% of the time, Pallas kernels for 0%

commit v1 on v0

--- a/solution.py
+++ b/solution.py
@@ -32,7 +32,9 @@
 
 
 def norm_rows(stream, gain):
-    whole = lax.all_gather(stream, "tp", axis=1, tiled=True)
+    count = lax.axis_size("tp")
+    repeats = [count if d == 1 else 1 for d in range(stream.ndim)]
+    whole = lax.all_to_all(jnp.tile(stream, repeats), "tp", split_axis=1, concat_axis=1, tiled=True)
     values = whole.astype(jnp.float32)
     scale = lax.rsqrt(jnp.mean(values * values, axis=1, keepdims=True) + epsilon)
     return (values * scale * gain).astype(jnp.bfloat16)

time: 432 us -> 409 us (0.947)
  waiting for transfers between devices: 328 us -> 267 us
  local copies, waits for them, and re-layouts: 6.23 us -> 26.7 us
  starting transfers between devices: 23 us -> 34.8 us
    all_gather x3, waiting for transfers between devices: 157 us -> 0.01 us  [sent_together(): lax.all_gather(both, axis, axis=dim, tiled=True)]
    all_to_all x0 -> x3, waiting for transfers between devices: none -> 112 us  [norm_rows(): lax.all_to_all(jnp.tile(stream, repeats), 'tp', split_axis=1, concat_axis...]
    all_gather x3 -> x0, waiting for transfers between devices: 63.2 us -> none  [norm_rows(): whole = lax.all_gather(stream, 'tp', axis=1, tiled=True)]
    all_to_all x3, waiting for transfers between devices: 0.01 us -> 51.2 us  [copy_for_each(): return lax.all_to_all(copies, axis, split_axis=0, concat_axis=0, tiled=True)]
    all_to_all x0 -> x3, starting transfers between devices: none -> 12.3 us  [norm_rows(): lax.all_to_all(jnp.tile(stream, repeats), 'tp', split_axis=1, concat_axis...]
    all_to_all x0 -> x3, local copies, waits for them, and re-layouts: none -> 9.56 us  [norm_rows(): lax.all_to_all(jnp.tile(stream, repeats), 'tp', split_axis=1, concat_axis...]
    another operation x0 -> x3, local copies, waits for them, and re-layouts: none -> 6.65 us  [norm_rows(): jnp.tile(stream, repeats)]
    convert_element_type x1 -> x3, other arithmetic: 0.79 us -> 7.37 us  [norm_rows(): return (values * scale * gain).astype(jnp.bfloat16)]
  transfers between devices with their start and end apart: 12 -> 12, of which waited for: 9 -> 8; matrix products, arithmetic and copies ran while one was open for 8% -> 13% of each run, Pallas kernels for 0% -> 0%
where the time goes in v1:
time: 409 us; the launch traced here: 408 us
  waiting for transfers between devices  267 us (65%)
  matrix products  46.9 us (11%)
  starting transfers between devices  34.8 us (9%)
  local copies, waits for them, and re-layouts  26.7 us (7%)
  other arithmetic  18.4 us (4%)
  between operations  13.7 us (3%)
    all_to_all x3, waiting for transfers between devices, norm_rows(): lax.all_to_all(jnp.tile(stream, repeats), 'tp', split_axis=1, concat_axis...  112 us
    reduce_scatter x3, waiting for transfers between devices, project_down(): lax.psum_scatter(partial_sum.astype(jnp.bfloat16), 'tp', scatter_dimensio...  104 us
    all_to_all x3, waiting for transfers between devices, copy_for_each(): return lax.all_to_all(copies, axis, split_axis=0, concat_axis=0, tiled=True)  51.2 us
    dot_general x3, matrix products, project_down(): jnp.dot(hidden, gathered_copies(weight, 'fs', 1), preferred_element_type=...  28.1 us
    all_to_all x3, starting transfers between devices, copy_for_each(): return lax.all_to_all(copies, axis, split_axis=0, concat_axis=0, tiled=True)  22 us
    dot_general x4, matrix products, add_rows(): return jnp.dot(gathered, piece, preferred_element_type=jnp.float32)  18.7 us
    all_to_all x3, starting transfers between devices, norm_rows(): lax.all_to_all(jnp.tile(stream, repeats), 'tp', split_axis=1, concat_axis...  12.3 us
    all_to_all x3, local copies, waits for them, and re-layouts, norm_rows(): lax.all_to_all(jnp.tile(stream, repeats), 'tp', split_axis=1, concat_axis...  9.56 us
  transfers between devices with their start and end apart: 12, of which 8 were waited for; matrix products, arithmetic and copies ran while one was open for 13% of the time, Pallas kernels for 0%

profile of v1, /device:TPU:0, one launch (start us, length us, event | category | flops | bytes accessed | tf_op | source)
XLA Modules:
  0.0 407.8 jit_solution(2424159184898974945)
XLA Ops:
  8.3 2.9 tile.6
  11.2 4.7 %all-to-all-start = ((bf16[768,8,256]{2,0,1:T(8,128)(2,1)}), bf16[768,8,256]{2,0,1:T(8,128)(2,1)S(1)}, u32[]{:S(2)}, u32[]{:S(2)}) async-start(bf16[768,8,256]{2,0,1:T(8,128)(2,1)} %tile.6), calls=%async_computation | async-start | bytes 6291456 | tf_op jit(solution)/shard_map/all_to_all | solution.py:37
  16.1 38.2 %all-to-all-done = bf16[768,8,256]{2,0,1:T(8,128)(2,1)S(1)} async-done(((bf16[768,8,256]{2,0,1:T(8,128)(2,1)}), bf16[768,8,256]{2,0,1:T(8,128)(2,1)S(1)}, u32[]{:S(2)}, u32[]{:S(2)}) %all-to-all-start) | async-done | bytes 3145760 | tf_op jit(solution)/shard_map/all_to_all | solution.py:37
  56.9 7.9 %all-to-all-start.1 = ((bf16[16,640,128]{1,2,0:T(8,128)(2,1)}), bf16[16,640,128]{1,2,0:T(8,128)(2,1)}, u32[]{:S(2)}, u32[]{:S(2)}) async-start(bf16[16,640,128]{1,2,0:T(8,128)(2,1)} %broadcast_in_dim.6), calls=%async_computation.1 | async-start | bytes 5242880 | tf_op jit(solution)/shard_map/all_to_all | solution.py:20
  64.9 3.2 copy.22
  71.3 6.8 %fusion.12 = f32[768,640]{1,0:T(8,128)} fusion(bf16[768,2048]{0,1:T(8,128)(2,1)} %fusion.5, bf16[2048,1280]{1,0:T(8,128)(2,1)} %all-gather.4.cloned.1.call-done), kind=kOutput, calls=%fused_computation.21 | convolution fusion | flops 2013265920 | bytes 7733248 | tf_op jit(solution)/shard_map/dot_general | solution.py:44
  78.1 25.7 %all-to-all-done.1 = bf16[16,640,128]{1,2,0:T(8,128)(2,1)} async-done(((bf16[16,640,128]{1,2,0:T(8,128)(2,1)}), bf16[16,640,128]{1,2,0:T(8,128)(2,1)}, u32[]{:S(2)}, u32[]{:S(2)}) %all-to-all-start.1) | async-done | bytes 2621472 | tf_op jit(solution)/shard_map/all_to_all | solution.py:20
  103.7 10.9 %convolution_convert_fusion.1 = bf16[768,2048]{1,0:T(8,128)(2,1)} fusion(bf16[640,2048]{0,1:T(8,128)(2,1)} %bitcast.3, f32[768,640]{1,0:T(8,128)} %fusion.12, bf16[768,2048]{0,1:T(8,128)(2,1)S(1)} %copy-done.6, bf16[2048,1280]{1,0:T(8,128)(2,1)} %all-gather.4.cloned.1.call-done), kind=kOutput, calls=%fused_computation.13 | convolution fusion | flops 4031053824 | bytes 13500416 | tf_op jit(solution)/shard_map/dot_general | solution.py:63
  114.7 36.3 %reduce-scatter.4.cloned.1.call-done = bf16[768,256]{1,0:T(8,128)(2,1)} async-done(((bf16[768,2048]{1,0:T(8,128)(2,1)}), bf16[768,256]{1,0:T(8,128)(2,1)}) %reduce-scatter.4.cloned.1.call-update) | async-done | bytes 393232 | tf_op jit(solution)/shard_map/reduce_scatter | solution.py:66
  153.9 3.8 all-to-all-start.2
  160.7 35.3 %all-to-all-done.2 = bf16[768,8,256]{2,0,1:T(8,128)(2,1)S(1)} async-done(((bf16[768,8,256]{2,0,1:T(8,128)(2,1)}), bf16[768,8,256]{2,0,1:T(8,128)(2,1)S(1)}, u32[]{:S(2)}, u32[]{:S(2)}) %all-to-all-start.2) | async-done | bytes 3145760 | tf_op jit(solution)/shard_map/all_to_all | solution.py:37
  197.8 7.1 %all-to-all-start.3 = ((bf16[16,128,128]{1,2,0:T(8,128)(2,1)}), bf16[16,128,128]{1,2,0:T(8,128)(2,1)}, u32[]{:S(2)}, u32[]{:S(2)}) async-start(bf16[16,128,128]{1,2,0:T(8,128)(2,1)} %broadcast_in_dim.7), calls=%async_computation.4 | async-start | bytes 1048576 | tf_op jit(solution)/shard_map/all_to_all | solution.py:20
  205.1 3.2 copy.24
  211.4 3.1 fusion.24
  217.5 6.4 %convolution_convert_fusion.2 = bf16[768,2048]{1,0:T(8,128)(2,1)} fusion(bf16[128,2048]{0,1:T(8,128)(2,1)} %bitcast.11, f32[768,128]{1,0:T(8,128)} %bitcast.50, bf16[768,2048]{0,1:T(8,128)(2,1)S(1)} %copy-done, bf16[2048,384]{1,0:T(8,128)(2,1)} %all-gather.6.cloned.1.call-done), kind=kOutput, calls=%fused_computation.14 | convolution fusion | flops 807075840 | bytes 7733248 | tf_op jit(solution)/shard_map/dot_general | solution.py:63
  225.7 34.0 %reduce-scatter.6.cloned.1.call-done = bf16[768,256]{1,0:T(8,128)(2,1)} async-done(((bf16[768,2048]{1,0:T(8,128)(2,1)}), bf16[768,256]{1,0:T(8,128)(2,1)}) %reduce-scatter.6.cloned.1.call-update) | async-done | bytes 393232 | tf_op jit(solution)/shard_map/reduce_scatter | solution.py:66
  263.4 3.8 all-to-all-start.4
  267.4 38.2 %all-to-all-done.4 = bf16[768,8,256]{2,0,1:T(8,128)(2,1)S(1)} async-done(((bf16[768,8,256]{2,0,1:T(8,128)(2,1)}), bf16[768,8,256]{2,0,1:T(8,128)(2,1)S(1)}, u32[]{:S(2)}, u32[]{:S(2)}) %all-to-all-start.4) | async-done | bytes 3145760 | tf_op jit(solution)/shard_map/all_to_all | solution.py:37
  308.1 7.0 %all-to-all-start.5 = ((bf16[16,640,128]{1,2,0:T(8,128)(2,1)}), bf16[16,640,128]{1,2,0:T(8,128)(2,1)}, u32[]{:S(2)}, u32[]{:S(2)}) async-start(bf16[16,640,128]{1,2,0:T(8,128)(2,1)} %broadcast_in_dim.8), calls=%async_computation.7 | async-start | bytes 5242880 | tf_op jit(solution)/shard_map/all_to_all | solution.py:20
  315.4 3.2 copy.26
  321.8 6.8 %fusion.8 = f32[768,640]{1,0:T(8,128)} fusion(bf16[768,2048]{0,1:T(8,128)(2,1)} %fusion.1, bf16[2048,1280]{1,0:T(8,128)(2,1)} %all-gather.8.cloned.1.call-done), kind=kOutput, calls=%fused_computation.17 | convolution fusion | flops 2013265920 | bytes 7733248 | tf_op jit(solution)/shard_map/dot_general | solution.py:44
  328.6 25.5 %all-to-all-done.5 = bf16[16,640,128]{1,2,0:T(8,128)(2,1)} async-done(((bf16[16,640,128]{1,2,0:T(8,128)(2,1)}), bf16[16,640,128]{1,2,0:T(8,128)(2,1)}, u32[]{:S(2)}, u32[]{:S(2)}) %all-to-all-start.5) | async-done | bytes 2621472 | tf_op jit(solution)/shard_map/all_to_all | solution.py:20
  354.0 10.9 %convolution_convert_fusion = bf16[768,2048]{1,0:T(8,128)(2,1)} fusion(bf16[640,2048]{0,1:T(8,128)(2,1)} %bitcast.14, f32[768,640]{1,0:T(8,128)} %fusion.8, bf16[768,2048]{0,1:T(8,128)(2,1)S(1)} %copy-done.7, bf16[2048,1280]{1,0:T(8,128)(2,1)} %all-gather.8.cloned.1.call-done), kind=kOutput, calls=%fused_computation.12 | convolution fusion | flops 4031053824 | bytes 13500416 | tf_op jit(solution)/shard_map/dot_general | solution.py:63
  365.0 34.1 %reduce-scatter.8.cloned.1.call-done = bf16[768,256]{1,0:T(8,128)(2,1)} async-done(((bf16[768,2048]{1,0:T(8,128)(2,1)}), bf16[768,256]{1,0:T(8,128)(2,1)}) %reduce-scatter.8.cloned.1.call-update) | async-done | bytes 393232 | tf_op jit(solution)/shard_map/reduce_scatter | solution.py:66
  (76 shorter events, 35.3 us)
Async XLA Ops:
  6.5 64.8 %all-gather.4.cloned.1.call-start = ((), (), s32[]{:S(2)}) async-start(), calls=%async_computation.9 | async-start | bytes 5570560 | tf_op jit(solution)/shard_map/all_gather | solution.py:15
  11.2 4.7 %copy-start.11 = (bf16[640,128]{1,0:T(8,128)(2,1)S(1)}, bf16[640,128]{1,0:T(8,128)(2,1)}, u32[]{:S(2)}) copy-start(bf16[640,128]{1,0:T(8,128)(2,1)} %param.19) | copy-start | bytes 491524
  11.2 43.1 %all-to-all-start = ((bf16[768,8,256]{2,0,1:T(8,128)(2,1)}), bf16[768,8,256]{2,0,1:T(8,128)(2,1)S(1)}, u32[]{:S(2)}, u32[]{:S(2)}) async-start(bf16[768,8,256]{2,0,1:T(8,128)(2,1)} %tile.6), calls=%async_computation | async-start | bytes 6291456 | tf_op jit(solution)/shard_map/all_to_all | solution.py:37
  54.3 2.6 copy-start.2
  56.9 46.8 %all-to-all-start.1 = ((bf16[16,640,128]{1,2,0:T(8,128)(2,1)}), bf16[16,640,128]{1,2,0:T(8,128)(2,1)}, u32[]{:S(2)}, u32[]{:S(2)}) async-start(bf16[16,640,128]{1,2,0:T(8,128)(2,1)} %broadcast_in_dim.6), calls=%async_computation.1 | async-start | bytes 5242880 | tf_op jit(solution)/shard_map/all_to_all | solution.py:20
  64.8 86.1 %reduce-scatter.4.cloned.1.call-start = ((), (), s32[]{:S(2)}) async-start(), calls=%async_computation.10 | async-start | bytes 3538944 | tf_op jit(solution)/shard_map/reduce_scatter | solution.py:66
  71.3 32.5 %copy-start.6 = (bf16[768,2048]{0,1:T(8,128)(2,1)S(1)}, bf16[768,2048]{0,1:T(8,128)(2,1)}, u32[]{:S(2)}) copy-start(bf16[768,2048]{0,1:T(8,128)(2,1)} %fusion.5) | copy-start | bytes 9437188
  114.6 36.3 %copy-start.8 = (bf16[2,384,256]{2,1,0:T(8,128)(2,1)S(1)}, bf16[2,384,256]{2,1,0:T(8,128)(2,1)}, u32[]{:S(2)}) copy-start(bf16[2,384,256]{2,1,0:T(8,128)(2,1)} %param.15) | copy-start | bytes 1179652
  153.9 6.8 %copy-start.16 = (f32[3,128]{1,0:T(4,128)S(1)}, f32[3,128]{1,0:T(4,128)}, u32[]{:S(2)}) copy-start(f32[3,128]{1,0:T(4,128)} %param.24) | copy-start | bytes 4612
  153.9 42.1 %all-to-all-start.2 = ((bf16[768,8,256]{2,0,1:T(8,128)(2,1)}), bf16[768,8,256]{2,0,1:T(8,128)(2,1)S(1)}, u32[]{:S(2)}, u32[]{:S(2)}) async-start(bf16[768,8,256]{2,0,1:T(8,128)(2,1)} %tile.7), calls=%async_computation.3 | async-start | bytes 6291456 | tf_op jit(solution)/shard_map/all_to_all | solution.py:37
  157.7 53.8 %all-gather.6.cloned.1.call-start = ((), (), s32[]{:S(2)}) async-start(), calls=%async_computation.11 | async-start | bytes 1671168 | tf_op jit(solution)/shard_map/all_gather | solution.py:15
  196.0 8.9 %copy-start.1 = (bf16[768,8,256]{2,0,1:T(8,128)(2,1)}, bf16[768,8,256]{2,0,1:T(8,128)(2,1)S(1)}, u32[]{:S(2)}) copy-start(bf16[768,8,256]{2,0,1:T(8,128)(2,1)S(1)} %all-to-all-done.2) | copy-start | bytes 9437188
  197.8 19.7 %all-to-all-start.3 = ((bf16[16,128,128]{1,2,0:T(8,128)(2,1)}), bf16[16,128,128]{1,2,0:T(8,128)(2,1)}, u32[]{:S(2)}, u32[]{:S(2)}) async-start(bf16[16,128,128]{1,2,0:T(8,128)(2,1)} %broadcast_in_dim.7), calls=%async_computation.4 | async-start | bytes 1048576 | tf_op jit(solution)/shard_map/all_to_all | solution.py:20
  204.9 54.8 %reduce-scatter.6.cloned.1.call-start = ((), (), s32[]{:S(2)}) async-start(), calls=%async_computation.12 | async-start | bytes 3538944 | tf_op jit(solution)/shard_map/reduce_scatter | solution.py:66
  211.4 3.2 copy-start
  223.9 1.0 copy-start.10
  223.9 97.8 %all-gather.8.cloned.1.call-start = ((), (), s32[]{:S(2)}) async-start(), calls=%async_computation.13 | async-start | bytes 5570560 | tf_op jit(solution)/shard_map/all_gather | solution.py:15
  263.4 3.8 copy-start.12
  263.4 42.1 %all-to-all-start.4 = ((bf16[768,8,256]{2,0,1:T(8,128)(2,1)}), bf16[768,8,256]{2,0,1:T(8,128)(2,1)S(1)}, u32[]{:S(2)}, u32[]{:S(2)}) async-start(bf16[768,8,256]{2,0,1:T(8,128)(2,1)} %tile.8), calls=%async_computation.6 | async-start | bytes 6291456 | tf_op jit(solution)/shard_map/all_to_all | solution.py:37
  305.6 2.6 copy-start.3
  308.1 45.9 %all-to-all-start.5 = ((bf16[16,640,128]{1,2,0:T(8,128)(2,1)}), bf16[16,640,128]{1,2,0:T(8,128)(2,1)}, u32[]{:S(2)}, u32[]{:S(2)}) async-start(bf16[16,640,128]{1,2,0:T(8,128)(2,1)} %broadcast_in_dim.8), calls=%async_computation.7 | async-start | bytes 5242880 | tf_op jit(solution)/shard_map/all_to_all | solution.py:20
  315.1 84.0 %reduce-scatter.8.cloned.1.call-start = ((), (), s32[]{:S(2)}) async-start(), calls=%async_computation.14 | async-start | bytes 3538944 | tf_op jit(solution)/shard_map/reduce_scatter | solution.py:66
  321.8 32.3 %copy-start.7 = (bf16[768,2048]{0,1:T(8,128)(2,1)S(1)}, bf16[768,2048]{0,1:T(8,128)(2,1)}, u32[]{:S(2)}) copy-start(bf16[768,2048]{0,1:T(8,128)(2,1)} %fusion.1) | copy-start | bytes 9437188
  364.9 34.2 %copy-start.5 = (bf16[768,256]{1,0:T(8,128)(2,1)S(1)}, bf16[768,256]{1,0:T(8,128)(2,1)}, u32[]{:S(2)}) copy-start(bf16[768,256]{1,0:T(8,128)(2,1)} %copy-done.4) | copy-start | bytes 1179652
  (5 other events, 3.8 us)
Sparse Core Ops, SparseCore 0:
  9.5 58.8 all-gather.3
  114.8 36.1 reduce-scatter.3
  160.6 45.5 all-gather.5
  224.1 35.5 reduce-scatter.5
  261.7 55.1 all-gather.7
  365.1 33.9 reduce-scatter.7
